TPU v7x, 32 devices: a whole 2x2x4 slice. The times are simulated.
32 devices in a mesh: dp: 2 (over x), kv: 8 (over z, y), tp: 2 (over core).
Axes of the slice: x: 2, y: 2, z: 4, core: 2. Of those that a mesh axis runs over, the one named last changes fastest.
Arguments:
- tokens: bfloat16 [32, 16, 2048], P('dp', None, ('kv', 'tp')), may hold values from -190 to 190
- gain_in: float32 [2048], P(('kv', 'tp')), may hold values from 0.1 to 1.9
- w_qdown: bfloat16 [2048, 512], P(('kv', 'tp')), may hold values from -0.125 to 0.125
- w_kvdown: bfloat16 [2048, 256], P(('kv', 'tp')), may hold values from -0.125 to 0.125
- w_ropek: bfloat16 [2048, 32], replicated, may hold values from -0.125 to 0.125
- gain_qlat: float32 [512], replicated, may hold values from 0.1 to 1.9
- gain_kvlat: float32 [256], replicated, may hold values from 0.1 to 1.9
- w_qup: bfloat16 [512, 16, 96], P(None, 'tp'), may hold values from -0.25 to 0.25
- gain_q: float32 [96], replicated, may hold values from 0.4 to 20
- w_ukey: bfloat16 [256, 16, 64], P(None, 'tp'), may hold values from -0.75 to 0.75
- w_uval: bfloat16 [256, 16, 128], P(None, 'tp'), may hold values from -0.375 to 0.375
- w_out: bfloat16 [2048, 2048], P('tp', 'kv'), may hold values from -2.5 to 2.5
- gain_out: float32 [2048], P(('kv', 'tp')), may hold values from 0.1 to 1.9
- cache_lat: bfloat16 [32, 2048, 256], P('dp', 'kv'), may hold values from -6 to 6
- cache_rope: bfloat16 [32, 32, 2048], P('dp', None, 'kv'), may hold values from -6 to 6
- parents: int32 [32, 16], P('dp'), may hold values from -1 to 14, as said below
- lengths: int32 [32], P('dp'), may hold values from 1024 to 2016
- accepted: int32 [32], P('dp'), may hold values from 0 to 16
Outputs:
- attn_out: bfloat16 [32, 16, 2048], P('dp', None, ('kv', 'tp'))
- lat_cache_out: bfloat16 [32, 2048, 256], P('dp', 'kv')
- rope_cache_out: bfloat16 [32, 32, 2048], P('dp', None, 'kv')
Inputs may be any that keep to these rules, and one draw needn't show every extreme that they name: `parents`: proposal j's parent is -1 (the last accepted token) or a proposal before j. Rows 0 .. lengths + accepted - 1 of a sequence's cache hold its past; the 16 positions after them lie inside the cache.
All inputs are finite; a program needn't handle non-finite values.
Results may differ from a plain program's by a relative error of at most 0.0102.
The roundings to bfloat16 on the way count: a program that leaves them out, or rounds other values in their place, can miss the bound.
Values may be sent and summed in bfloat16 or wider, within the bound.
A program may use at most 64 MiB of HBM per device.

v0:
```python
import jax
import jax.numpy as jnp
from jax import lax
from jax.sharding import PartitionSpec as P

epsilon = 1e-06


def normed(values, gain_vec):
    return (
        values * lax.rsqrt(jnp.mean(values * values, axis=-1, keepdims=True) + epsilon) * gain_vec
    )


def rope_angles(position, half_dim):
    frequency = 10000.0 ** (-(jnp.arange(half_dim, dtype=jnp.float32) * 2.0) / (2 * half_dim))
    return position.astype(jnp.float32)[..., None] * frequency


def ancestry(parents):
    proposals = parents.shape[-1]
    parent_link = (parents[..., :, None] == jnp.arange(proposals, dtype=jnp.int32)).astype(
        jnp.float32
    )
    identity = jnp.broadcast_to(jnp.eye(proposals, dtype=jnp.float32), parent_link.shape)

    def extend(iteration, state_pair):
        reaches, current = state_pair
        current = jnp.einsum("sij,sjk->sik", current, parent_link, precision=lax.Precision.HIGHEST)
        return (reaches + current, current)

    reaches, current = lax.fori_loop(0, proposals - 1, extend, (identity, identity))
    depths = (jnp.sum(reaches, axis=-1) - 1.0).astype(jnp.int32)
    return (reaches, depths)


def latents(summed, squares, full_width, gain_qlat, gain_kvlat):
    qrank = gain_qlat.shape[0]
    kvrank = gain_kvlat.shape[0]
    scaled_rows = summed * lax.rsqrt(squares / full_width + epsilon)[:, None]
    query_latent = normed(scaled_rows[:, :qrank], gain_qlat).astype(jnp.bfloat16)
    new_latent = normed(scaled_rows[:, qrank : qrank + kvrank], gain_kvlat).astype(jnp.bfloat16)
    new_rope = scaled_rows[:, qrank + kvrank :].astype(jnp.bfloat16)
    return (query_latent, new_latent, new_rope)


def apply_values(numer_rows, value_map):
    return jnp.einsum("...hk,khv->...hv", numer_rows, value_map, precision=lax.Precision.HIGHEST)


def local(
    tokens,
    gain_in,
    w_qdown,
    w_kvdown,
    w_ropek,
    gain_qlat,
    gain_kvlat,
    w_qup,
    gain_q,
    w_ukey,
    w_uval,
    w_out,
    gain_out,
    cache_lat,
    cache_rope,
    parents,
    lengths,
    accepted,
):
    seq_count, proposals, local_width = tokens.shape
    full_width = local_width * lax.axis_size(("kv", "tp"))
    tok_rows = tokens.astype(jnp.float32).reshape(seq_count * proposals, local_width)
    scaled = (tok_rows * gain_in).astype(jnp.bfloat16)
    squares = jnp.sum(tok_rows * tok_rows, axis=-1)
    rope_rows = lax.dynamic_slice_in_dim(
        w_ropek, lax.axis_index(("kv", "tp")) * local_width, local_width, 0
    )
    joined = jnp.concatenate([w_qdown, w_kvdown, rope_rows], axis=1)
    partial_rows = jnp.dot(scaled, joined, preferred_element_type=jnp.float32)
    summed, total_squares = lax.psum((partial_rows, squares), ("kv", "tp"))
    query_latent, new_latent, new_rope = latents(
        summed, total_squares, full_width, gain_qlat, gain_kvlat
    )
    qrank = w_qup.shape[0]
    heads_here = w_qup.shape[1]
    qkhead = w_qup.shape[2]
    kvrank = w_ukey.shape[0]
    nope_dim = w_ukey.shape[2]
    vhead = w_uval.shape[2]
    rope_dim = cache_rope.shape[1]
    half_dim = rope_dim // 2
    reaches, depths = ancestry(parents)
    starts = lengths + accepted
    query_pos = starts[:, None] + depths
    queries = jnp.dot(
        query_latent, w_qup.reshape(qrank, heads_here * qkhead), preferred_element_type=jnp.float32
    )
    queries = normed(queries.reshape(seq_count, proposals, heads_here, qkhead), gain_q)
    query_nope = queries[..., :nope_dim].astype(jnp.bfloat16)
    angles = rope_angles(query_pos, half_dim)[:, :, None, :]
    cosine = jnp.cos(angles)
    sines = jnp.sin(angles)
    lower_half = queries[..., nope_dim : nope_dim + half_dim]
    upper_half = queries[..., nope_dim + half_dim :]
    query_rot = jnp.concatenate(
        [lower_half * cosine - upper_half * sines, upper_half * cosine + lower_half * sines],
        axis=-1,
    ).astype(jnp.bfloat16)
    query_lat = jnp.einsum(
        "sihn,khn->sihk", query_nope, w_ukey, preferred_element_type=jnp.float32
    ).astype(jnp.bfloat16)
    pos_count = cache_lat.shape[1]
    slots = lax.axis_index("kv") * pos_count + jnp.arange(pos_count, dtype=jnp.int32)
    offset = slots[None, :] - starts[:, None]
    inside = (offset >= 0) & (offset < proposals)
    matches = offset[:, :, None] == jnp.arange(proposals, dtype=jnp.int32)
    selector = matches.astype(jnp.bfloat16)
    new_latent = new_latent.reshape(seq_count, proposals, kvrank)
    new_rope = new_rope.reshape(seq_count, proposals, rope_dim)
    placed = jnp.einsum(
        "spj,sjk->spk", selector, new_latent, preferred_element_type=jnp.float32
    ).astype(jnp.bfloat16)
    lat_out = jnp.where(inside[:, :, None], placed, cache_lat)
    placed_rope = jnp.einsum(
        "spj,sjr->srp", selector, new_rope, preferred_element_type=jnp.float32
    ).astype(jnp.bfloat16)
    rope_out = jnp.where(inside[:, None, :], placed_rope, cache_rope)
    key_pos = jnp.where(
        inside,
        starts[:, None] + jnp.sum(jnp.where(matches, depths[:, None, :], 0), axis=-1),
        slots[None, :],
    )
    ancestor = jnp.einsum(
        "sij,spj->sip", reaches, matches.astype(jnp.float32), precision=lax.Precision.HIGHEST
    )
    visible = (offset < 0)[:, None, :] | (ancestor > 0.5)
    key_angles = jnp.swapaxes(rope_angles(key_pos, half_dim), 1, 2)
    key_cos = jnp.cos(key_angles)
    key_sin = jnp.sin(key_angles)
    rope32 = rope_out.astype(jnp.float32)
    key_low = rope32[:, :half_dim, :]
    key_high = rope32[:, half_dim:, :]
    key_rot = jnp.concatenate(
        [key_low * key_cos - key_high * key_sin, key_high * key_cos + key_low * key_sin], axis=1
    ).astype(jnp.bfloat16)
    scores = (
        jnp.einsum("sihk,spk->sihp", query_lat, lat_out, preferred_element_type=jnp.float32)
        + jnp.einsum("sihr,srp->sihp", query_rot, key_rot, preferred_element_type=jnp.float32)
    ) * qkhead ** (-0.5)
    masked = jnp.where(visible[:, :, None, :], scores, -jnp.inf)
    row_max = lax.pmax(jnp.max(masked, axis=-1), "kv")
    weights32 = jnp.exp(masked - row_max[..., None])
    denominator = jnp.sum(weights32, axis=-1)
    weights = weights32.astype(jnp.bfloat16)
    numerator = jnp.einsum("sihp,spk->sihk", weights, lat_out, preferred_element_type=jnp.float32)
    value_map = w_uval.astype(jnp.float32)
    numer_values = apply_values(numerator, value_map)
    values_all, denom_all = lax.psum((numer_values, denominator), "kv")
    head_out = (values_all / denom_all[..., None]).astype(jnp.bfloat16)
    head_rows = head_out.reshape(seq_count * proposals, heads_here * vhead)
    partial_out = jnp.dot(head_rows, w_out, preferred_element_type=jnp.float32).reshape(
        seq_count, proposals, w_out.shape[1]
    )
    mixed = lax.psum_scatter(partial_out, "tp", scatter_dimension=2, tiled=True)
    local_squares = jnp.sum(mixed * mixed, axis=-1)
    norm_total = lax.psum(local_squares, ("kv", "tp"))
    result = (mixed * lax.rsqrt(norm_total / full_width + epsilon)[..., None] * gain_out).astype(
        jnp.bfloat16
    )
    return (result, lat_out, rope_out)


def solution(mesh):
    placed = (
        P("dp", None, ("kv", "tp")),
        P(("kv", "tp")),
        P(("kv", "tp"), None),
        P(("kv", "tp"), None),
        P(),
        P(),
        P(),
        P(None, "tp", None),
        P(),
        P(None, "tp", None),
        P(None, "tp", None),
        P("tp", "kv"),
        P(("kv", "tp")),
        P("dp", "kv", None),
        P("dp", None, "kv"),
        P("dp", None),
        P("dp"),
        P("dp"),
    )
    return jax.shard_map(
        local,
        mesh=mesh,
        in_specs=placed,
        out_specs=(P("dp", None, ("kv", "tp")), P("dp", "kv", None), P("dp", None, "kv")),
        check_vma=False,
    )
```

profile of v0, /device:TPU:0, one launch (start us, length us, event | category | flops | bytes accessed | tf_op | source)
XLA Modules:
  0.0 292.3 jit_solution(4244914604734968146)
XLA Ops:
  7.3 0.8 constant_dynamic-slice_fusion
  8.2 0.9 fusion.43
  9.0 2.2 fusion.37
  11.7 5.6 %while.13 = (s32[]{:T(128)}, f32[16,16,16]{2,1,0:T(8,128)S(1)}, f32[16,16,16]{2,1,0:T(8,128)S(1)}, s32[16,16]{1,0:T(8,128)S(1)}, s32[]{:T(128)}) while((s32[]{:T(128)}, f32[16,16,16]{2,1,0:T(8,128)S(1)}, f32[16,16,16]{2,1,0:T(8,128)S(1)}, s32[16,16]{1,0:T(8,128)S(1)}, s32[]{:T(128)}) %tuple.45), condition=%wide.region_1.0_spmd.clone, body=%wide.region_0.0_spmd.clone.sunk | while | flops 798722 | bytes 99389 | solution.py:32
  17.6 35.1 %psum.36 = f32[256]{0:T(256)S(1)} all-reduce(f32[256]{0:T(256)S(1)} %reduce_sum.75), channel_id=1, replica_groups=mesh['dp'=2,'kv'=8,'tp'=2] {'kv','tp'}, use_global_device_ids=true, to_apply=%region_4.0 | all-reduce | flops 256 | bytes 2048 | tf_op jit(solution)/shard_map/psum | solution.py:81
  53.7 53.2 %all-reduce.3.cloned.1.call-done = f32[256,800]{0,1:T(8,128)} async-done(((f32[256,800]{0,1:T(8,128)}), f32[256,800]{0,1:T(8,128)}) %all-reduce.3.cloned.1.call-update) | async-done | bytes 819216 | tf_op jit(solution)/shard_map/psum | solution.py:81
  107.0 1.2 broadcast_multiply_fusion
  109.7 1.0 fusion.52
  110.7 1.1 fusion.31
  112.6 0.6 subtract_convert_fusion
  113.5 0.7 copy-done.2
  114.2 1.4 convert_select_fusion
  115.6 0.9 fusion.5
  116.5 2.0 fusion.53
  118.5 37.9 %pmax.7 = f32[16,16,8]{2,1,0:T(8,128)S(1)} all-reduce(f32[16,16,8]{2,1,0:T(8,128)S(1)} %get-tuple-element.61), channel_id=1, replica_groups=mesh['dp'=2,'kv'=8,'tp'=2] {'kv'}, use_global_device_ids=true, to_apply=%region_11.12 | all-reduce | flops 2048 | bytes 16384 | tf_op jit(solution)/shard_map/pmax | solution.py:152
  156.4 2.3 fusion.9
  159.7 2.1 convolution_bitcast_fusion
  161.9 35.7 %psum.38 = f32[16,16,8]{2,1,0:T(8,128)S(1)} all-reduce(f32[16,16,8]{2,1,0:T(8,128)S(1)} %get-tuple-element.47), channel_id=1, replica_groups=mesh['dp'=2,'kv'=8,'tp'=2] {'kv'}, use_global_device_ids=true, to_apply=%region_14.15 | all-reduce | flops 2048 | bytes 16384 | tf_op jit(solution)/shard_map/psum | solution.py:159
  197.8 41.0 %all-reduce.5.cloned.1.call-done = f32[16,16,8,128]{3,1,0,2:T(8,128)} async-done(((f32[16,16,8,128]{3,1,0,2:T(8,128)}), f32[16,16,8,128]{3,1,0,2:T(8,128)}) %all-reduce.5.cloned.1.call-update) | async-done | bytes 1048592 | tf_op jit(solution)/shard_map/psum | solution.py:159
  238.8 2.4 fusion.18
  241.2 7.5 %reduce-scatter.2.cloned.1.call-done = f32[16,16,128]{2,1,0:T(8,128)} async-done(((f32[16,16,256]{2,1,0:T(8,128)}), f32[16,16,128]{2,1,0:T(8,128)}) %reduce-scatter.2.cloned.1.call-update) | async-done | bytes 131088 | tf_op jit(solution)/shard_map/reduce_scatter | solution.py:165
  248.7 1.0 multiply_reduce_fusion.3
  249.7 34.4 %psum.39 = f32[16,16]{1,0:T(8,128)S(1)} all-reduce(f32[16,16]{1,0:T(8,128)S(1)} %multiply_reduce_fusion.3), channel_id=1, replica_groups=mesh['dp'=2,'kv'=8,'tp'=2] {'kv','tp'}, use_global_device_ids=true, to_apply=%region_17.18 | all-reduce | flops 256 | bytes 2048 | tf_op jit(solution)/shard_map/psum | solution.py:167
  284.1 1.6 multiply_convert_fusion.2
  (102 shorter events, 10.7 us)
Async XLA Ops:
  7.2 101.8 %copy-start = (bf16[512,8,96]{0,2,1:T(8,128)(2,1)S(1)}, bf16[512,8,96]{0,2,1:T(8,128)(2,1)}, u32[]{:S(2)}) copy-start(bf16[512,8,96]{0,2,1:T(8,128)(2,1)} %param.27) | copy-start | bytes 2359300
  7.2 4.1 %copy-start.6 = (bf16[16,16,128]{2,1,0:T(8,128)(2,1)S(1)}, bf16[16,16,128]{2,1,0:T(8,128)(2,1)}, u32[]{:S(2)}) copy-start(bf16[16,16,128]{2,1,0:T(8,128)(2,1)} %param.20) | copy-start | bytes 196612
  7.2 4.2 %copy-start.14 = (s32[16]{0:T(128)S(1)}, s32[16]{0:T(128)}, u32[]{:S(2)}) copy-start(s32[16]{0:T(128)} %param.37) | copy-start | bytes 196
  7.2 4.2 %copy-start.13 = (s32[16]{0:T(128)S(1)}, s32[16]{0:T(128)}, u32[]{:S(2)}) copy-start(s32[16]{0:T(128)} %param.36) | copy-start | bytes 196
  7.2 4.4 %copy-start.7 = (s32[16,16]{1,0:T(8,128)S(1)}, s32[16,16]{1,0:T(8,128)}, u32[]{:S(2)}) copy-start(s32[16,16]{1,0:T(8,128)} %param.35) | copy-start | bytes 3076
  7.2 99.7 %all-reduce.3.cloned.1.call-start = ((), (), s32[]{:S(2)}) async-start(), calls=%async_computation.1 | async-start | bytes 1638400 | tf_op jit(solution)/shard_map/psum | solution.py:81
  11.2 227.5 %all-reduce.5.cloned.1.call-start = ((), (), s32[]{:S(2)}) async-start(), calls=%async_computation.2 | async-start | bytes 2097152 | tf_op jit(solution)/shard_map/psum | solution.py:159
  17.3 91.2 %copy-start.8 = (f32[512]{0:T(512)S(1)}, f32[512]{0:T(512)}, u32[]{:S(2)}) copy-start(f32[512]{0:T(512)} %param.25) | copy-start | bytes 6148
  53.0 55.8 %copy-start.9 = (f32[256]{0:T(256)S(1)}, f32[256]{0:T(256)}, u32[]{:S(2)}) copy-start(f32[256]{0:T(256)} %param.26) | copy-start | bytes 3076
  108.5 1.2 copy-start.4
  109.0 2.8 copy-start.10
  109.6 2.5 copy-start.5
  112.6 1.6 copy-start.2
  115.6 43.1 %copy-start.1 = (bf16[16,256,256]{2,1,0:T(8,128)(2,1)}, bf16[16,256,256]{2,1,0:T(8,128)(2,1)S(1)}, u32[]{:S(2)}) copy-start(bf16[16,256,256]{2,1,0:T(8,128)(2,1)S(1)} %convert_select_fusion) | copy-start | bytes 6291460
  158.7 1.0 copy-start.3
  159.7 79.0 %copy-start.12 = (bf16[1024,256]{1,0:T(8,128)(2,1)S(1)}, bf16[1024,256]{1,0:T(8,128)(2,1)}, u32[]{:S(2)}) copy-start(bf16[1024,256]{1,0:T(8,128)(2,1)} %param.31) | copy-start | bytes 1572868
  161.9 86.8 %reduce-scatter.2.cloned.1.call-start = ((), (), s32[]{:S(2)}) async-start(), calls=%async_computation.3 | async-start | bytes 393216 | tf_op jit(solution)/shard_map/reduce_scatter | solution.py:165
  197.8 86.3 %copy-start.11 = (f32[128]{0:T(128)S(1)}, f32[128]{0:T(128)}, u32[]{:S(2)}) copy-start(f32[128]{0:T(128)} %param.32) | copy-start | bytes 1540
Sparse Core Ops, SparseCore 0:
  12.1 94.8 all-reduce.2
  162.0 76.7 all-reduce.4
  241.3 7.3 reduce-scatter.1
where the time goes:
time: 293 us; the launch traced here: 292 us
  blocking collectives  143 us (49%)
  waiting for transfers between devices  102 us (35%)
  matrix products  18.7 us (6%)
  between operations  14.2 us (5%)
  other arithmetic  11 us (4%)
    psum x1, waiting for transfers between devices, local(): summed, total_squares = lax.psum((partial_rows, squares), ('kv', 'tp'))  53.2 us
    psum x1, waiting for transfers between devices, local(): values_all, denom_all = lax.psum((numer_values, denominator), 'kv')  41 us
    pmax x1, blocking collectives, local(): row_max = lax.pmax(jnp.max(masked, axis=-1), 'kv')  37.9 us
    psum x1, blocking collectives, local(): values_all, denom_all = lax.psum((numer_values, denominator), 'kv')  35.7 us
    psum x1, blocking collectives, local(): summed, total_squares = lax.psum((partial_rows, squares), ('kv', 'tp'))  35.1 us
    psum x1, blocking collectives, local(): norm_total = lax.psum(local_squares, ('kv', 'tp'))  34.4 us
    reduce_scatter x1, waiting for transfers between devices, local(): mixed = lax.psum_scatter(partial_out, 'tp', scatter_dimension=2, tiled=True)  7.5 us
  transfers between devices with their start and end apart: 3, of which 3 were waited for; matrix products, arithmetic and copies ran while one was open for 2% of the time, Pallas kernels for 0%

commit v1 on v0

--- a/solution.py
+++ b/solution.py
@@ -1,6 +1,10 @@
+import functools
+
 import jax
 import jax.numpy as jnp
 from jax import lax
+from jax.experimental import pallas as pl
+from jax.experimental.pallas import tpu as pltpu
 from jax.sharding import PartitionSpec as P
 
 epsilon = 1e-06
@@ -48,7 +52,482 @@
     return jnp.einsum("...hk,khv->...hv", numer_rows, value_map, precision=lax.Precision.HIGHEST)
 
 
-def local(
+MESH = pl.DeviceIdType.MESH
+
+
+def remote(src, dst, send_sem, recv_sem, kv, tp):
+    return pltpu.make_async_remote_copy(
+        src_ref=src,
+        dst_ref=dst,
+        send_sem=send_sem,
+        recv_sem=recv_sem,
+        device_id={"kv": kv, "tp": tp},
+        device_id_type=MESH,
+    )
+
+
+def greet(nkv, ntp, me_kv, me_tp):
+    barrier = pltpu.get_barrier_semaphore()
+    for step in range(1, nkv * ntp):
+        kv = lax.rem(me_kv + step // ntp, nkv)
+        tp = lax.rem(me_tp + step % ntp, ntp)
+        pl.semaphore_signal(barrier, inc=1, device_id={"kv": kv, "tp": tp}, device_id_type=MESH)
+    return barrier
+
+
+def visit_order(nz):
+    return [nz // 2] + [step for step in range(1, nz) if step != nz // 2] + [0]
+
+
+def latent_kernel(
+    nkv,
+    tok_ref,
+    gin_ref,
+    wq_ref,
+    wkv_ref,
+    wr_ref,
+    gq_ref,
+    gk_ref,
+    qlat_ref,
+    nlat_ref,
+    nrope_ref,
+    wpad,
+    part,
+    xbuf,
+    sbuf,
+    ybuf,
+    zbuf,
+    rbuf,
+    gbuf,
+    xsems,
+    ysend,
+    yrecv,
+    zsend,
+    zrecv,
+    gsend,
+    grecv,
+    ysend2,
+    fsend,
+):
+    ntp, ny = 2, 2
+    nz = nkv // ny
+    me_kv, me_tp = lax.axis_index("kv"), lax.axis_index("tp")
+    me_z, me_y = me_kv // ny, lax.rem(me_kv, ny)
+    other = 1 - me_tp
+    mate = me_z * ny + (1 - me_y)
+    barrier = greet(nkv, ntp, me_kv, me_tp)
+    rows, width = tok_ref.shape
+    each = rows // (nkv * ntp)
+    qr, kr, rd = wq_ref.shape[1], wkv_ref.shape[1], wr_ref.shape[0]
+    full = width * nkv * ntp
+
+    tok = tok_ref[...].astype(jnp.float32)
+    scaled = (tok * gin_ref[...]).astype(jnp.bfloat16)
+    squares = jnp.sum(tok * tok, axis=-1, keepdims=True)
+    wpad[...] = jnp.zeros_like(wpad)
+    first = pl.multiple_of((me_kv * ntp + me_tp) * width, width)
+    wpad[:rd, :] = wr_ref[:, pl.ds(first, width)]
+    pq = jnp.dot(scaled, wq_ref[...], preferred_element_type=jnp.float32)
+    pk = jnp.dot(scaled, wkv_ref[...], preferred_element_type=jnp.float32)
+    pr = lax.dot_general(
+        scaled, wpad[...], (((1,), (1,)), ((), ())), preferred_element_type=jnp.float32
+    )
+    lane = lax.broadcasted_iota(jnp.int32, pr.shape, 1)
+    pr = jnp.where(lane == rd, squares, pr)
+    for block in range(nkv * ntp):
+        kv, tp = block // ntp, block % ntp
+        span = slice(block * each, (block + 1) * each)
+        part[tp, kv, :, :qr] = pq[span]
+        part[tp, kv, :, qr : qr + kr] = pk[span]
+        part[tp, kv, :, qr + kr :] = pr[span]
+
+    pl.semaphore_wait(barrier, nkv * ntp - 1)
+    swap = remote(part.at[other], xbuf, xsems.at[0], xsems.at[1], me_kv, other)
+    swap.start()
+    swap.wait()
+    small = lax.broadcasted_iota(jnp.int32, (each, 128), 1)
+    for kv in range(nkv):
+        sbuf[kv] = part[me_tp, kv] + xbuf[kv]
+    sends = []
+    order = visit_order(nz)
+
+    def to_mate(z):
+        return remote(
+            sbuf.at[z * ny + 1 - me_y], ybuf.at[z], ysend.at[z], yrecv.at[z], mate, me_tp
+        )
+
+    for step in order:
+        copy = to_mate(lax.rem(me_z + step, nz))
+        copy.start()
+        sends.append(copy)
+    for step in order:
+        z = lax.rem(me_z + step, nz)
+        to_mate(z).wait_recv()
+        acc = sbuf[z * ny + me_y] + ybuf[z]
+        if step:
+            zbuf[z] = acc
+            copy = remote(
+                zbuf.at[z],
+                rbuf.at[me_z],
+                zsend.at[z],
+                zrecv.at[me_z],
+                z * ny + me_y,
+                me_tp,
+            )
+            copy.start()
+            sends.append(copy)
+    for step in range(1, nz):
+        z = lax.rem(me_z + step, nz)
+        remote(
+            zbuf.at[z], rbuf.at[z], zsend.at[z], zrecv.at[z], z * ny + me_y, me_tp
+        ).wait_recv()
+        acc = acc + rbuf[z]
+    ends = acc[:, qr + kr :]
+    square = ends[:, rd : rd + 1]
+    scale = lax.rsqrt(square / full + epsilon)
+    zq = acc[:, :qr] * scale
+    zk = acc[:, qr : qr + kr] * scale
+    mine = me_kv * ntp + me_tp
+    gbuf[mine, :, :qr] = normed(zq, gq_ref[...]).astype(jnp.bfloat16)
+    gbuf[mine, :, qr : qr + kr] = normed(zk, gk_ref[...]).astype(jnp.bfloat16)
+    gbuf[mine, :, qr + kr :] = (ends * scale).astype(jnp.bfloat16)
+
+    def pass_on(slot, sem, kv, tp):
+        return remote(gbuf.at[slot], gbuf.at[slot], sem, grecv.at[slot], kv, tp)
+
+    for step in order[:-1]:
+        z = lax.rem(me_z + step, nz)
+        copy = pass_on(mine, gsend.at[step], z * ny + me_y, me_tp)
+        copy.start()
+        sends.append(copy)
+    for step in range(nz):
+        kv = lax.rem(me_z + step, nz) * ny + me_y
+        slot = kv * ntp + me_tp
+        if step:
+            pass_on(slot, gsend.at[step], kv, me_tp).wait_recv()
+        for copy in (
+            pass_on(slot, ysend2.at[step], mate, me_tp),
+            pass_on(slot, fsend.at[step], me_kv, other),
+        ):
+            copy.start()
+            sends.append(copy)
+    for step in range(nz):
+        kv = lax.rem(me_z + step, nz) * ny + 1 - me_y
+        slot = kv * ntp + me_tp
+        pass_on(slot, ysend2.at[step], mate, me_tp).wait_recv()
+        copy = pass_on(slot, fsend.at[nz + step], me_kv, other)
+        copy.start()
+        sends.append(copy)
+    for step in range(nkv):
+        kv = lax.rem(me_kv + step, nkv)
+        slot = kv * ntp + other
+        pass_on(slot, fsend.at[step], me_kv, other).wait_recv()
+    for copy in sends:
+        copy.wait_send()
+    for block in range(nkv * ntp):
+        span = slice(block * each, (block + 1) * each)
+        qlat_ref[span, :] = gbuf[block, :, :qr]
+        nlat_ref[span, :] = gbuf[block, :, qr : qr + kr]
+        nrope_ref[span, :] = gbuf[block, :, qr + kr : qr + kr + rd]
+
+
+def gather_latents(nkv, tokens, gain_in, w_qdown, w_kvdown, w_ropek, gain_qlat, gain_kvlat):
+    rows = tokens.shape[0]
+    each = rows // (nkv * 2)
+    qr, kr, rd = w_qdown.shape[1], w_kvdown.shape[1], w_ropek.shape[1]
+    nz = nkv // 2
+    wide = qr + kr + 128
+    vmem = pl.BlockSpec(memory_space=pltpu.VMEM)
+    dma = pltpu.SemaphoreType.DMA
+    return pl.pallas_call(
+        functools.partial(latent_kernel, nkv),
+        out_shape=(
+            jax.ShapeDtypeStruct((rows, qr), jnp.bfloat16),
+            jax.ShapeDtypeStruct((rows, kr), jnp.bfloat16),
+            jax.ShapeDtypeStruct((rows, rd), jnp.bfloat16),
+        ),
+        in_specs=[vmem] * 7,
+        out_specs=(vmem, vmem, vmem),
+        scratch_shapes=[
+            pltpu.VMEM((128, tokens.shape[1]), jnp.bfloat16),
+            pltpu.VMEM((2, nkv, each, wide), jnp.float32),
+            pltpu.VMEM((nkv, each, wide), jnp.float32),
+            pltpu.VMEM((nkv, each, wide), jnp.float32),
+            pltpu.VMEM((nz, each, wide), jnp.float32),
+            pltpu.VMEM((nz, each, wide), jnp.float32),
+            pltpu.VMEM((nz, each, wide), jnp.float32),
+            pltpu.VMEM((nkv * 2, each, wide), jnp.bfloat16),
+            dma((2,)),
+            dma((nz,)),
+            dma((nz,)),
+            dma((nz,)),
+            dma((nz,)),
+            dma((nz,)),
+            dma((nkv * 2,)),
+            dma((nz,)),
+            dma((nkv,)),
+        ],
+        compiler_params=pltpu.CompilerParams(
+            collective_id=1, has_side_effects=True, vmem_limit_bytes=48 * 1024 * 1024
+        ),
+    )(tokens, gain_in[None], w_qdown, w_kvdown, w_ropek.T, gain_qlat[None], gain_kvlat[None])
+
+
+def output_kernel(
+    nkv,
+    heads,
+    val_ref,
+    stat_ref,
+    wout_ref,
+    gout_ref,
+    out_ref,
+    ystat,
+    mstat,
+    zstat,
+    scol,
+    ybuf,
+    zbuf,
+    rbuf,
+    obuf,
+    pbuf,
+    xbuf,
+    nbuf,
+    tsems,
+    ysend,
+    yrecv,
+    tsend,
+    trecv,
+    zsend,
+    zrecv,
+    osend,
+    orecv,
+    fsend,
+    xsems,
+    nsend,
+    nrecv,
+):
+    ntp, ny = 2, 2
+    nz = nkv // ny
+    me_kv, me_tp = lax.axis_index("kv"), lax.axis_index("tp")
+    me_z, me_y = me_kv // ny, lax.rem(me_kv, ny)
+    other = 1 - me_tp
+    mate = me_z * ny + (1 - me_y)
+    barrier = greet(nkv, ntp, me_kv, me_tp)
+    pl.semaphore_wait(barrier, nkv * ntp - 1)
+    _, each, channels = val_ref.shape
+    vhead = channels // heads
+    order = visit_order(nz)
+    span = nz * each
+
+    def columns(parts, at):
+        stacked = jnp.concatenate(parts, axis=0)
+        rest = jnp.zeros((128 - stacked.shape[0], span), jnp.float32)
+        turned = jnp.concatenate([stacked, rest], axis=0).T
+        for z in range(nz):
+            scol[at, z] = turned[z * each : (z + 1) * each]
+
+    def to_mate(z):
+        return remote(
+            val_ref.at[z * ny + 1 - me_y], ybuf.at[z], ysend.at[z], yrecv.at[z], mate, me_tp
+        )
+
+    stat_copy = remote(stat_ref.at[1 - me_y], ystat, tsems.at[0], tsems.at[1], mate, me_tp)
+    stat_copy.start()
+    sends = []
+    for step in order:
+        copy = to_mate(lax.rem(me_z + step, nz))
+        copy.start()
+        sends.append(copy)
+    stat_copy.wait()
+    here, there = stat_ref[me_y], ystat[...]
+    top = jnp.maximum(here[:heads], there[:heads])
+    here_scale = jnp.exp(here[:heads] - top)
+    there_scale = jnp.exp(there[:heads] - top)
+    mstat[:heads] = top
+    mstat[heads:] = here[heads:] * here_scale + there[heads:] * there_scale
+
+    def stat_to(step):
+        kv = lax.rem(me_z + step, nz) * ny + me_y
+        return remote(mstat, zstat.at[me_z], tsend.at[step], trecv.at[me_z], kv, me_tp)
+
+    columns([here_scale, there_scale], 0)
+    for step in order[:-1]:
+        copy = stat_to(step)
+        copy.start()
+        sends.append(copy)
+    for step in order:
+        z = lax.rem(me_z + step, nz)
+        to_mate(z).wait_recv()
+        factors = scol[0, z]
+        acc = []
+        for head in range(heads):
+            lanes = slice(head * vhead, (head + 1) * vhead)
+            term = val_ref[z * ny + me_y, :, lanes].astype(jnp.float32) * factors[
+                :, head : head + 1
+            ] + ybuf[z, :, lanes].astype(jnp.float32) * factors[
+                :, heads + head : heads + head + 1
+            ]
+            if step:
+                zbuf[z, :, lanes] = term.astype(jnp.bfloat16)
+            acc.append(term)
+        if step:
+            copy = remote(
+                zbuf.at[z], rbuf.at[me_z], zsend.at[z], zrecv.at[me_z], z * ny + me_y, me_tp
+            )
+            copy.start()
+            sends.append(copy)
+    stats = [mstat[...]]
+    for step in range(1, nz):
+        z = lax.rem(me_z + step, nz)
+        remote(
+            mstat, zstat.at[z], tsend.at[step], trecv.at[z], z * ny + me_y, me_tp
+        ).wait_recv()
+        stats.append(zstat[z])
+    top = functools.reduce(jnp.maximum, [stat[:heads] for stat in stats])
+    scales = [jnp.exp(stat[:heads] - top) for stat in stats]
+    total = sum(scale * stat[heads:] for scale, stat in zip(scales, stats))
+    columns(scales + [total], 1)
+    factors = scol[1, me_z]
+    acc = [term * factors[:, head : head + 1] for head, term in enumerate(acc)]
+    for step in range(1, nz):
+        z = lax.rem(me_z + step, nz)
+        remote(
+            zbuf.at[z], rbuf.at[z], zsend.at[z], zrecv.at[z], z * ny + me_y, me_tp
+        ).wait_recv()
+        for head in range(heads):
+            at = step * heads + head
+            acc[head] = acc[head] + (
+                rbuf[z, :, head * vhead : (head + 1) * vhead].astype(jnp.float32)
+                * factors[:, at : at + 1]
+            )
+    for head in range(heads):
+        at = nz * heads + head
+        obuf[me_kv, :, head * vhead : (head + 1) * vhead] = (
+            acc[head] / factors[:, at : at + 1]
+        ).astype(jnp.bfloat16)
+
+    def gather_to(slot, sem, kv):
+        return remote(obuf.at[slot], obuf.at[slot], sem, orecv.at[slot], kv, me_tp)
+
+    for step in range(1, nz):
+        kv = lax.rem(me_z + step, nz) * ny + me_y
+        copy = gather_to(me_kv, osend.at[step], kv)
+        copy.start()
+        sends.append(copy)
+    for step in range(nz):
+        slot = lax.rem(me_z + step, nz) * ny + me_y
+        if step:
+            gather_to(slot, osend.at[step], slot).wait_recv()
+        copy = gather_to(slot, fsend.at[step], mate)
+        copy.start()
+        sends.append(copy)
+    for step in range(nz):
+        slot = lax.rem(me_z + step, nz) * ny + (1 - me_y)
+        gather_to(slot, fsend.at[step], mate).wait_recv()
+
+    half = wout_ref.shape[1] // ntp
+    joined = obuf[...].reshape(nkv * each, channels)
+    partial_out = jnp.dot(joined, wout_ref[...], preferred_element_type=jnp.float32)
+    low, high = partial_out[:, :half], partial_out[:, half:]
+    pbuf[...] = jnp.where(me_tp == 0, high, low)
+    swap = remote(pbuf, xbuf, xsems.at[0], xsems.at[1], me_kv, other)
+    swap.start()
+    kept = jnp.where(me_tp == 0, low, high)
+    swap.wait()
+    mixed = kept + xbuf[...]
+    ones = jnp.ones((8, half), jnp.float32)
+    local_squares = lax.dot_general(
+        ones,
+        mixed * mixed,
+        (((1,), (1,)), ((), ())),
+        precision=lax.Precision.HIGHEST,
+        preferred_element_type=jnp.float32,
+    )
+    mine = me_kv * ntp + me_tp
+    nbuf[mine] = local_squares[:1]
+    for step in range(1, nkv * ntp):
+        kv = lax.rem(me_kv + step // ntp, nkv)
+        tp = lax.rem(me_tp + step % ntp, ntp)
+        copy = remote(nbuf.at[mine], nbuf.at[mine], nsend.at[step], nrecv.at[mine], kv, tp)
+        copy.start()
+        sends.append(copy)
+    for step in range(1, nkv * ntp):
+        kv = lax.rem(me_kv + step // ntp, nkv)
+        tp = lax.rem(me_tp + step % ntp, ntp)
+        slot = kv * ntp + tp
+        remote(
+            nbuf.at[slot], nbuf.at[slot], nsend.at[step], nrecv.at[slot], kv, tp
+        ).wait_recv()
+    norm = nbuf[0]
+    for slot in range(1, nkv * ntp):
+        norm = norm + nbuf[slot]
+    full = half * ntp * nkv
+    factor = lax.rsqrt(norm / full + epsilon)
+    factor = jnp.broadcast_to(factor, (half, nkv * each)).T
+    out_ref[...] = (mixed * factor * gout_ref[...]).astype(jnp.bfloat16)
+    for copy in sends:
+        copy.wait_send()
+
+
+def project_output(nkv, heads, values, stats, w_out, gain_out):
+    _, each, channels = values.shape
+    half = w_out.shape[1] // 2
+    rows = nkv * each
+    nz = nkv // 2
+    vmem = pl.BlockSpec(memory_space=pltpu.VMEM)
+    dma = pltpu.SemaphoreType.DMA
+    return pl.pallas_call(
+        functools.partial(output_kernel, nkv, heads),
+        out_shape=jax.ShapeDtypeStruct((rows, half), jnp.bfloat16),
+        in_specs=[vmem] * 4,
+        out_specs=vmem,
+        scratch_shapes=[
+            pltpu.VMEM((2 * heads, nz * each), jnp.float32),
+            pltpu.VMEM((2 * heads, nz * each), jnp.float32),
+            pltpu.VMEM((nz, 2 * heads, nz * each), jnp.float32),
+            pltpu.VMEM((2, nz, each, 128), jnp.float32),
+            pltpu.VMEM((nz, each, channels), jnp.bfloat16),
+            pltpu.VMEM((nz, each, channels), jnp.bfloat16),
+            pltpu.VMEM((nz, each, channels), jnp.bfloat16),
+            pltpu.VMEM((nkv, each, channels), jnp.bfloat16),
+            pltpu.VMEM((rows, half), jnp.float32),
+            pltpu.VMEM((rows, half), jnp.float32),
+            pltpu.VMEM((nkv * 2, 1, rows), jnp.float32),
+            dma((2,)),
+            dma((nz,)),
+            dma((nz,)),
+            dma((nz,)),
+            dma((nz,)),
+            dma((nz,)),
+            dma((nz,)),
+            dma((nz,)),
+            dma((nkv,)),
+            dma((nz,)),
+            dma((2,)),
+            dma((nkv * 2,)),
+            dma((nkv * 2,)),
+        ],
+        compiler_params=pltpu.CompilerParams(
+            collective_id=2, has_side_effects=True, vmem_limit_bytes=48 * 1024 * 1024
+        ),
+    )(values, stats, w_out, gain_out[None])
+
+
+def ancestry_fast(parents):
+    proposals = parents.shape[-1]
+    link = (parents[..., :, None] == jnp.arange(proposals, dtype=jnp.int32)).astype(jnp.bfloat16)
+    reaches = link + jnp.eye(proposals, dtype=jnp.bfloat16)
+    span = 2
+    while span < proposals:
+        link = jnp.einsum("sij,sjk->sik", link, link)
+        reaches = reaches + jnp.einsum("sij,sjk->sik", reaches, link)
+        span *= 2
+    reaches = reaches.astype(jnp.float32)
+    depths = (jnp.sum(reaches, axis=-1) - 1.0).astype(jnp.int32)
+    return (reaches, depths)
+
+
+def local_plain(
     tokens,
     gain_in,
     w_qdown,
@@ -171,6 +650,126 @@
     return (result, lat_out, rope_out)
 
 
+def local_fast(
+    tokens,
+    gain_in,
+    w_qdown,
+    w_kvdown,
+    w_ropek,
+    gain_qlat,
+    gain_kvlat,
+    w_qup,
+    gain_q,
+    w_ukey,
+    w_uval,
+    w_out,
+    gain_out,
+    cache_lat,
+    cache_rope,
+    parents,
+    lengths,
+    accepted,
+):
+    seq_count, proposals, local_width = tokens.shape
+    nkv = lax.axis_size("kv")
+    query_latent, new_latent, new_rope = gather_latents(
+        nkv,
+        tokens.reshape(seq_count * proposals, local_width),
+        gain_in,
+        w_qdown,
+        w_kvdown,
+        w_ropek,
+        gain_qlat,
+        gain_kvlat,
+    )
+    qrank = w_qup.shape[0]
+    heads_here = w_qup.shape[1]
+    qkhead = w_qup.shape[2]
+    kvrank = w_ukey.shape[0]
+    nope_dim = w_ukey.shape[2]
+    vhead = w_uval.shape[2]
+    rope_dim = cache_rope.shape[1]
+    half_dim = rope_dim // 2
+    reaches, depths = ancestry_fast(parents)
+    starts = lengths + accepted
+    query_pos = starts[:, None] + depths
+    queries = jnp.dot(
+        query_latent, w_qup.reshape(qrank, heads_here * qkhead), preferred_element_type=jnp.float32
+    )
+    queries = normed(queries.reshape(seq_count, proposals, heads_here, qkhead), gain_q)
+    query_nope = queries[..., :nope_dim].astype(jnp.bfloat16)
+    angles = rope_angles(query_pos, half_dim)[:, :, None, :]
+    cosine = jnp.cos(angles)
+    sines = jnp.sin(angles)
+    lower_half = queries[..., nope_dim : nope_dim + half_dim]
+    upper_half = queries[..., nope_dim + half_dim :]
+    query_rot = jnp.concatenate(
+        [lower_half * cosine - upper_half * sines, upper_half * cosine + lower_half * sines],
+        axis=-1,
+    ).astype(jnp.bfloat16)
+    query_lat = jnp.einsum(
+        "sihn,khn->sihk", query_nope, w_ukey, preferred_element_type=jnp.float32
+    ).astype(jnp.bfloat16)
+    pos_count = cache_lat.shape[1]
+    slots = lax.axis_index("kv") * pos_count + jnp.arange(pos_count, dtype=jnp.int32)
+    offset = slots[None, :] - starts[:, None]
+    inside = (offset >= 0) & (offset < proposals)
+    matches = offset[:, :, None] == jnp.arange(proposals, dtype=jnp.int32)
+    selector = matches.astype(jnp.bfloat16)
+    new_latent = new_latent.reshape(seq_count, proposals, kvrank)
+    new_rope = new_rope.reshape(seq_count, proposals, rope_dim)
+    placed = jnp.einsum(
+        "spj,sjk->spk", selector, new_latent, preferred_element_type=jnp.float32
+    ).astype(jnp.bfloat16)
+    lat_out = jnp.where(inside[:, :, None], placed, cache_lat)
+    placed_rope = jnp.einsum(
+        "spj,sjr->srp", selector, new_rope, preferred_element_type=jnp.float32
+    ).astype(jnp.bfloat16)
+    rope_out = jnp.where(inside[:, None, :], placed_rope, cache_rope)
+    key_pos = jnp.where(
+        inside,
+        starts[:, None] + jnp.sum(jnp.where(matches, depths[:, None, :], 0), axis=-1),
+        slots[None, :],
+    )
+    ancestor = jnp.einsum(
+        "sij,spj->sip", reaches, matches.astype(jnp.float32), precision=lax.Precision.HIGHEST
+    )
+    visible = (offset < 0)[:, None, :] | (ancestor > 0.5)
+    key_angles = jnp.swapaxes(rope_angles(key_pos, half_dim), 1, 2)
+    key_cos = jnp.cos(key_angles)
+    key_sin = jnp.sin(key_angles)
+    rope32 = rope_out.astype(jnp.float32)
+    key_low = rope32[:, :half_dim, :]
+    key_high = rope32[:, half_dim:, :]
+    key_rot = jnp.concatenate(
+        [key_low * key_cos - key_high * key_sin, key_high * key_cos + key_low * key_sin], axis=1
+    ).astype(jnp.bfloat16)
+    scores = (
+        jnp.einsum("sihk,spk->sihp", query_lat, lat_out, preferred_element_type=jnp.float32)
+        + jnp.einsum("sihr,srp->sihp", query_rot, key_rot, preferred_element_type=jnp.float32)
+    ) * qkhead ** (-0.5)
+    masked = jnp.where(visible[:, :, None, :], scores, -1e30)
+    row_max = jnp.max(masked, axis=-1)
+    weights32 = jnp.exp(masked - row_max[..., None])
+    denominator = jnp.sum(weights32, axis=-1)
+    weights = weights32.astype(jnp.bfloat16)
+    numerator = jnp.einsum("sihp,spk->sihk", weights, lat_out, preferred_element_type=jnp.float32)
+    numer_values = apply_values(numerator, w_uval.astype(jnp.float32)).astype(jnp.bfloat16)
+    each = seq_count * proposals // nkv
+    stats = jnp.concatenate([row_max, denominator], axis=-1)
+    stats = stats.reshape(nkv // 2, 2, each, 2 * heads_here).transpose(1, 3, 0, 2)
+    stats = stats.reshape(2, 2 * heads_here, nkv // 2 * each)
+    result = project_output(
+        nkv,
+        heads_here,
+        numer_values.reshape(nkv, each, heads_here * vhead),
+        stats,
+        w_out,
+        gain_out,
+    )
+    return (result.reshape(seq_count, proposals, local_width), lat_out, rope_out)
+
+
 def solution(mesh):
     placed = (
         P("dp", None, ("kv", "tp")),
@@ -192,6 +791,17 @@
         P("dp"),
         P("dp"),
     )
+    nkv, ntp = mesh.shape["kv"], mesh.shape["tp"]
+
+    def local(*args):
+        tokens, w_qup, w_uval = args[0], args[7], args[10]
+        rows = tokens.shape[0] * tokens.shape[1]
+        fits = ntp == 2 and nkv % 2 == 0 and rows % (16 * nkv * ntp) == 0
+        heads = w_qup.shape[1]
+        fits = fits and rows % 256 == 0 and (nkv // 2 + 1) * heads <= 128 and heads % 8 == 0
+        fits = fits and tokens.shape[2] % 128 == 0 and w_uval.shape[2] % 128 == 0
+        return (local_fast if fits else local_plain)(*args)
+
     return jax.shard_map(
         local,
         mesh=mesh,

time: 293 us -> 84.3 us (0.29)
  blocking collectives: 143 us -> 0 us
  waiting for transfers between devices: 102 us -> 0 us
  Pallas kernels: 0 us -> 58.4 us
  between operations: 14.2 us -> 0.95 us
  matrix products: 18.7 us -> 10.6 us
  other arithmetic: 11 us -> 5.62 us
  local copies, waits for them, and re-layouts: 2.92 us -> 8.16 us
    psum x3 -> x0, blocking collectives: 105 us -> none  [the longest x1 35.7 us: local(): values_all, denom_all = lax.psum((numer_values, denominator), 'kv')]
    psum x2 -> x0, waiting for transfers between devices: 94.2 us -> none  [the longest x1 53.2 us: local(): summed, total_squares = lax.psum((partial_rows, squares), ('kv', 'tp'))]
    pallas_call x0 -> x2, Pallas kernels: none -> 58.4 us  [the longest x1 32.1 us: project_output(): pl.pallas_call(functools.partial(output_kernel, nkv, heads), out_shape=ja...]
    pmax x1 -> x0, blocking collectives: 37.9 us -> none  [local(): row_max = lax.pmax(jnp.max(masked, axis=-1), 'kv')]
    dot_general x25 -> x12, matrix products: 16.6 us -> 8.56 us  [the longest x1 1.74 us: local_fast(): jnp.einsum('sihp,spk->sihk', weights, lat_out, preferred_element_type=jnp...]
    reduce_scatter x1 -> x0, waiting for transfers between devices: 7.5 us -> none  [local(): mixed = lax.psum_scatter(partial_out, 'tp', scatter_dimension=2, tiled=True)]
    unnamed x30 -> x33, local copies, waits for them, and re-layouts: 1.31 us -> 7.37 us
  transfers between devices with their start and end apart: 3 -> 0, of which waited for: 3 -> 0; matrix products, arithmetic and copies ran while one was open for 2% -> 0% of each run, Pallas kernels for 0% -> 0%
where the time goes in v1:
time: 84.3 us; the launch traced here: 83.8 us
  Pallas kernels  58.4 us (69%)
  matrix products  10.6 us (13%)
  local copies, waits for them, and re-layouts  8.16 us (10%)
  other arithmetic  5.62 us (7%)
  between operations  0.95 us (1%)
    pallas_call x1, Pallas kernels, project_output(): pl.pallas_call(functools.partial(output_kernel, nkv, heads), out_shape=ja...  32.1 us
    pallas_call x1, Pallas kernels, gather_latents(): pl.pallas_call(functools.partial(latent_kernel, nkv), out_shape=(jax.Shap...  26.3 us
    unnamed x33, local copies, waits for them, and re-layouts  7.37 us
    another operation x2, other arithmetic  1.76 us
    dot_general x1, matrix products, local_fast(): jnp.einsum('sihp,spk->sihk', weights, lat_out, preferred_element_type=jnp...  1.74 us

profile of v1, /device:TPU:0, one launch (start us, length us, event | category | flops | bytes accessed | tf_op | source)
XLA Modules:
  0.0 83.8 jit_solution(2056845610778895454)
XLA Ops:
  0.7 0.8 add.83
  1.6 1.0 %convolution_convert_fusion.3 = bf16[16,16,16]{2,1,0:T(8,128)(2,1)S(1)} fusion(s32[16,16]{1,0:T(8,128)} %param.33), kind=kOutput, calls=%fused_computation.17 | convolution fusion | flops 147456 | bytes 9216
  2.6 0.9 %convolution_add_fusion.2 = bf16[16,16,16]{1,2,0:T(8,128)(2,1)S(1)} fusion(bf16[16,16,16]{2,1,0:T(8,128)(2,1)S(1)} %convolution_convert_fusion.3, s32[16,16]{1,0:T(8,128)} %param.33, bf16[16,16]{0,1:T(8,128)(2,1)S(1)} %fusion.41), kind=kOutput, calls=%fused_computation.19 | convolution fusion | flops 159744 | bytes 17920 | tf_op jit(solution)/shard_map/sij,sjk->sik/dot_general | solution.py:523
  5.3 0.9 %copy-done.2 = bf16[128,512]{1,0:T(8,128)(2,1)S(1)} copy-done((bf16[128,512]{1,0:T(8,128)(2,1)S(1)}, bf16[128,512]{1,0:T(8,128)(2,1)}, u32[]{:S(2)}) %copy-start.2) | copy-done | bytes 131096
  6.2 0.9 %copy-done.3 = bf16[2048,32]{0,1:T(8,128)(2,1)S(1)} copy-done((bf16[2048,32]{0,1:T(8,128)(2,1)S(1)}, bf16[2048,32]{0,1:T(8,128)(2,1)}, u32[]{:S(2)}) %copy-start.3) | copy-done | bytes 131096
  7.1 0.8 copy-done.4
  8.0 0.8 copy-done.5
  8.8 0.7 copy-done.6
  9.5 0.7 copy-done.7
  10.2 0.7 copy-done.8
  10.8 26.3 %shard_map.193 = (bf16[256,512]{1,0:T(8,128)(2,1)S(1)}, bf16[256,256]{1,0:T(8,128)(2,1)S(1)}, bf16[256,32]{1,0:T(8,128)(2,1)S(1)}) custom-call(bf16[256,128]{1,0:T(8,128)(2,1)S(1)} %bitcast.70, f32[1,128]{1,0:T(1,128)S(1)} %bitcast.74, bf16[128,512]{1,0:T(8,128)(2,1)S(1)} %copy-done.2, bf16[128,256]{1,0:T(8,128)(2,1)S(1)} %copy-done.5, ...), custom_call_target="tpu_custom_call" | custom-call | tf_op jit(solution)/shard_map/pallas_call | solution.py:242
  37.1 1.0 %fusion.43 = (f32[16,32,256]{2,1,0:T(8,128)S(1)}, bf16[16,32,256]{2,1,0:T(8,128)(2,1)}) fusion(bf16[16,32,256]{2,1,0:T(8,128)(2,1)S(1)} %copy-done.13, bf16[16,16,32]{2,1,0:T(8,128)(2,1)S(1)} %bitcast.71, s32[16,256]{1,0:T(8,128)S(1)} %broadcast_subtract_fusion, pred[16,256]{1,0:T(8,128)(4,1)S(1)} %get-tuple-element.18), kind=kOutput, calls=%fused_computation.78 | convolution fusion | flops 4653056 | bytes 1085440 | tf_op jit(solution)/shard_map/spj,sjr->srp/dot_general | solution.py:725
  38.1 1.1 %fusion.24 = (bf16[16,16,256]{2,1,0:T(8,128)(2,1)S(1)}, bf16[16,16,256]{2,1,0:T(8,128)(2,1)S(1)}) fusion(f32[16,32,256]{2,1,0:T(8,128)S(1)} %get-tuple-element.23, f32[16]{0:T(128)S(1)} %multiply_power_fusion, f32[16,256]{1,0:T(8,128)S(1)} %select_convert_fusion), kind=kLoop, calls=%fused_computation.42 | loop fusion | flops 589824 | bytes 802880 | tf_op jit(solution)/shard_map/convert
  39.3 0.6 multiply_reduce_fusion
  40.3 0.6 subtract_convert_fusion
  42.0 0.9 %copy-done.11 = bf16[16,256,256]{2,1,0:T(8,128)(2,1)S(1)} copy-done((bf16[16,256,256]{2,1,0:T(8,128)(2,1)S(1)}, bf16[16,256,256]{2,1,0:T(8,128)(2,1)}, u32[]{:S(2)}) %copy-start.11) | copy-done | bytes 2097176
  42.8 1.3 %convert_select_fusion = bf16[16,256,256]{2,1,0:T(8,128)(2,1)S(1)} fusion(bf16[16,256,256]{2,1,0:T(8,128)(2,1)S(1)} %copy-done.11, pred[16,256]{1,0:T(8,128)(4,1)S(1)} %get-tuple-element.18, bf16[16,16,256]{2,1,0:T(8,128)(2,1)S(1)} %bitcast.68, s32[16,256]{1,0:T(8,128)S(1)} %broadcast_subtract_fusion), kind=kOutput, calls=%fused_computation.6 | convolution fusion | flops 35717120 | bytes 4345856 | tf_op jit(solution)/shard_map/spj,sjk->spk/dot_general | solution.py:721
  44.1 0.9 %fusion = f32[16,16,8,256]{3,2,1,0:T(8,128)S(1)} fusion(bf16[16,256,256]{2,1,0:T(8,128)(2,1)S(1)} %convert_select_fusion, bf16[16,16,8,256]{3,1,0,2:T(8,128)(2,1)S(1)} %fusion.6), kind=kOutput, calls=%fused_computation | convolution fusion | flops 268435456 | bytes 5242880 | tf_op jit(solution)/shard_map/sihk,spk->sihp/dot_general | solution.py:748
  45.0 0.8 fusion.44
  45.8 1.4 %fusion.4 = (f32[16,16,8]{2,1,0:T(8,128)S(1)}, bf16[16,16,8,256]{3,2,1,0:T(8,128)(2,1)}) fusion(f32[16,16,8,256]{3,2,1,0:T(8,128)S(1)} %get-tuple-element.26, f32[16,16,8]{2,1,0:T(8,128)S(1)} %get-tuple-element.25), kind=kLoop, calls=%fused_computation.7 | loop fusion | flops 1570816 | bytes 3162112 | tf_op jit(solution)/shard_map/reduce_sum | solution.py:754
  47.5 1.7 %fusion.2 = f32[16,16,8,256]{3,1,0,2:T(8,128)S(1)} fusion(bf16[16,256,256]{2,1,0:T(8,128)(2,1)S(1)} %convert_select_fusion, bf16[16,16,8,256]{3,2,1,0:T(8,128)(2,1)} %get-tuple-element.10), kind=kOutput, calls=%fused_computation.2 | convolution fusion | flops 268435456 | bytes 5242880 | tf_op jit(solution)/shard_map/sihp,spk->sihk/dot_general | solution.py:756
  49.3 1.1 %fusion.7 = bf16[16,16,8,128]{3,1,0,2:T(8,128)(2,1)S(1)} fusion(f32[16,16,8,256]{3,1,0,2:T(8,128)S(1)} %fusion.2, bf16[256,8,128,1]{2,1,0,3:T(8,128)(2,1)S(1)} %bitcast.77), kind=kOutput, calls=%fused_computation.12 | convolution fusion | flops 805568512 | bytes 3145728 | tf_op jit(solution)/shard_map/...hk,khv->...hv/dot_general | solution.py:52
  51.0 32.1 %shard_map.194 = bf16[256,128]{1,0:T(8,128)(2,1)S(1)} custom-call(bf16[8,32,1024]{2,1,0:T(8,128)(2,1)S(1)} %reshape.252.val_ref, f32[2,16,128]{2,1,0:T(8,128)S(1)} %reshape.254.stat_ref, bf16[1024,256]{1,0:T(8,128)(2,1)S(1)} %copy-done.1, f32[1,128]{1,0:T(1,128)S(1)} %bitcast.75), custom_call_target="tpu_custom_call" | custom-call | tf_op jit(solution)/shard_map/pallas_call | solution.py:479
  83.1 0.6 copy.92
  (48 shorter events, 4.3 us)
Async XLA Ops:
  0.6 38.7 %copy-start = (bf16[512,8,96]{0,2,1:T(8,128)(2,1)S(1)}, bf16[512,8,96]{0,2,1:T(8,128)(2,1)}, u32[]{:S(2)}) copy-start(bf16[512,8,96]{0,2,1:T(8,128)(2,1)} %param.25) | copy-start | bytes 2359300
  0.6 36.5 %copy-start.13 = (bf16[16,32,256]{2,1,0:T(8,128)(2,1)S(1)}, bf16[16,32,256]{2,1,0:T(8,128)(2,1)}, u32[]{:S(2)}) copy-start(bf16[16,32,256]{2,1,0:T(8,128)(2,1)} %param.32) | copy-start | bytes 786436
  5.3 0.9 %copy-start.2 = (bf16[128,512]{1,0:T(8,128)(2,1)S(1)}, bf16[128,512]{1,0:T(8,128)(2,1)}, u32[]{:S(2)}) copy-start(bf16[128,512]{1,0:T(8,128)(2,1)} %wq_ref.1) | copy-start | bytes 393220
  6.2 0.9 %copy-start.3 = (bf16[2048,32]{0,1:T(8,128)(2,1)S(1)}, bf16[2048,32]{0,1:T(8,128)(2,1)}, u32[]{:S(2)}) copy-start(bf16[2048,32]{0,1:T(8,128)(2,1)} %param.22) | copy-start | bytes 393220
  7.1 0.8 %copy-start.4 = (bf16[16,16,128]{2,1,0:T(8,128)(2,1)S(1)}, bf16[16,16,128]{2,1,0:T(8,128)(2,1)}, u32[]{:S(2)}) copy-start(bf16[16,16,128]{2,1,0:T(8,128)(2,1)} %param.18) | copy-start | bytes 196612
  8.0 0.8 %copy-start.5 = (bf16[128,256]{1,0:T(8,128)(2,1)S(1)}, bf16[128,256]{1,0:T(8,128)(2,1)}, u32[]{:S(2)}) copy-start(bf16[128,256]{1,0:T(8,128)(2,1)} %wkv_ref.1) | copy-start | bytes 196612
  8.8 0.7 copy-start.6
  9.5 0.7 copy-start.7
  10.2 0.7 copy-start.8
  37.1 2.8 %copy-start.15 = (f32[96]{0:T(128)S(1)}, f32[96]{0:T(128)}, u32[]{:S(2)}) copy-start(f32[96]{0:T(128)} %param.26) | copy-start | bytes 1156
  40.3 1.0 %copy-start.14 = (bf16[256,8,64]{0,2,1:T(8,128)(2,1)S(1)}, bf16[256,8,64]{0,2,1:T(8,128)(2,1)}, u32[]{:S(2)}) copy-start(bf16[256,8,64]{0,2,1:T(8,128)(2,1)} %param.27) | copy-start | bytes 786436
  41.2 1.6 %copy-start.11 = (bf16[16,256,256]{2,1,0:T(8,128)(2,1)S(1)}, bf16[16,256,256]{2,1,0:T(8,128)(2,1)}, u32[]{:S(2)}) copy-start(bf16[16,256,256]{2,1,0:T(8,128)(2,1)} %param.31) | copy-start | bytes 6291460
  44.1 3.4 %copy-start.10 = (bf16[16,256,256]{2,1,0:T(8,128)(2,1)}, bf16[16,256,256]{2,1,0:T(8,128)(2,1)S(1)}, u32[]{:S(2)}) copy-start(bf16[16,256,256]{2,1,0:T(8,128)(2,1)S(1)} %convert_select_fusion) | copy-start | bytes 6291460
  47.5 1.8 %copy-start.12 = (bf16[256,8,128]{2,1,0:T(8,128)(2,1)S(1)}, bf16[256,8,128]{2,1,0:T(8,128)(2,1)}, u32[]{:S(2)}) copy-start(bf16[256,8,128]{2,1,0:T(8,128)(2,1)} %param.28) | copy-start | bytes 1572868
  49.3 1.7 %copy-start.1 = (bf16[1024,256]{1,0:T(8,128)(2,1)S(1)}, bf16[1024,256]{1,0:T(8,128)(2,1)}, u32[]{:S(2)}) copy-start(bf16[1024,256]{1,0:T(8,128)(2,1)} %wout_ref.1) | copy-start | bytes 1572868
  49.3 1.7 %copy-start.9 = (f32[128]{0:T(128)S(1)}, f32[128]{0:T(128)}, u32[]{:S(2)}) copy-start(f32[128]{0:T(128)} %param.30) | copy-start | bytes 1540
